TPU v7x, 32 devices: a whole 2x2x4 slice. The times are simulated.
32 devices in a mesh: sp: 16 (over z, y, x), tp: 2 (over core).
Axes of the slice: x: 2, y: 2, z: 4, core: 2. Of those that a mesh axis runs over, the one named last changes fastest.
Arguments:
- residual: bfloat16 [2048, 2048], P(('sp', 'tp')), may hold values from -6 to 6
- query_wide: bfloat16 [2048, 1024], P('sp', 'tp'), may hold values from -6 to 6
- key_wide: bfloat16 [2048, 1024], P('sp', 'tp'), may hold values from -6 to 6
- value_wide: bfloat16 [2048, 2048], P('sp', 'tp'), may hold values from -6 to 6
- outgate_wide: bfloat16 [2048, 2048], P('sp', 'tp'), may hold values from -6 to 6
- gating_wide: float32 [3, 8, 2048], P(None, 'tp', 'sp'), may hold values from -4 to 240, as said below
- gain_wide: bfloat16 [2048], P('tp'), may hold values from 0.099609375 to 1.8984375
- readout_wide: bfloat16 [2048, 2048], P('tp'), may hold values from -0.109375 to 0.109375
- query_narrow: bfloat16 [2048, 512], P('sp', 'tp'), may hold values from -6 to 6
- key_narrow: bfloat16 [2048, 512], P('sp', 'tp'), may hold values from -6 to 6
- value_narrow: bfloat16 [2048, 1024], P('sp', 'tp'), may hold values from -6 to 6
- outgate_narrow: bfloat16 [2048, 1024], P('sp', 'tp'), may hold values from -6 to 6
- gating_narrow: float32 [3, 8, 2048], P(None, 'tp', 'sp'), may hold values from -4 to 240, as said below
- gain_narrow: bfloat16 [1024], P('tp'), may hold values from 0.099609375 to 1.8984375
- readout_narrow: bfloat16 [1024, 2048], P('tp'), may hold values from -0.109375 to 0.109375
- norm_gain: bfloat16 [2048], replicated, may hold values from 0.099609375 to 1.8984375
- gate_weight: bfloat16 [2048, 5632], P('sp', 'tp'), may hold values from -0.125 to 0.125
- up_weight: bfloat16 [2048, 5632], P('sp', 'tp'), may hold values from -0.125 to 0.125
- down_weight: bfloat16 [5632, 2048], P('tp', 'sp'), may hold values from -0.078125 to 0.078125
Outputs:
- mixed_out: bfloat16 [2048, 2048], P(('sp', 'tp'))
Inputs may be any that keep to these rules, and one draw needn't show every extreme that they name: `gating_wide`: row 0 holds input gate pre-activations, row 1 forget gate pre-activations, row 2 an added log-decay that is zero or negative. `gating_narrow`: row 0 holds input gate pre-activations, row 1 forget gate pre-activations, row 2 an added log-decay that is zero or negative.
All inputs are finite; a program needn't handle non-finite values.
Results may differ from a plain program's by a relative error of at most 0.017.
Values may be sent and summed in bfloat16 or wider, within the bound.
No kernel may reach another device: no remote copies, remote signals or barrier semaphores. Data moves between devices by JAX's collectives and lax.ppermute only.
A program may use at most 128 MiB of HBM per device.

v0:
```python
import jax
import jax.numpy as jnp
from jax import lax
from jax.sharding import PartitionSpec as P

DK_A = 128
DK_B = 64
BLOCK = 64


def entering(value, axis, combine, identity):
    length, here = (lax.axis_size(axis), lax.axis_index(axis))
    everything = jax.tree.map(lambda part: lax.all_gather(part, axis), value)
    start = jax.tree.map(
        lambda part, zero: jnp.broadcast_to(jnp.asarray(zero, part.dtype), part.shape),
        value,
        identity,
    )

    def step(k, before):
        reached = k < here
        new = combine(before, jax.tree.map(lambda part: part[k], everything))
        return jax.tree.map(lambda a, b: jnp.where(reached, a, b), new, before)

    return lax.fori_loop(0, length, step, start)


def local_pass(query, key_rows, value, gating, key_size):
    rows = query.shape[0]
    attention_tally = gating.shape[1]
    value_size = value.shape[1] // attention_tally
    nblocks = rows // BLOCK
    scale = key_size ** (-0.5)
    queries = query.reshape(nblocks, BLOCK, attention_tally, key_size)
    keys_all = key_rows.reshape(nblocks, BLOCK, attention_tally, key_size)
    values_all = value.reshape(nblocks, BLOCK, attention_tally, value_size)
    incoming_matrix = jnp.moveaxis(gating[0].reshape(attention_tally, nblocks, BLOCK), 1, 0)
    forget_log = jax.nn.log_sigmoid(gating[1]) + gating[2]
    forgets = jnp.moveaxis(forget_log.reshape(attention_tally, nblocks, BLOCK), 1, 0)
    causal = jnp.tril(jnp.ones((BLOCK, BLOCK), dtype=bool))

    def advance(carry, blocks):
        memory, level = carry
        q_block, k_block, v_block, in_block, f_block = blocks
        cumul = jnp.cumsum(f_block, axis=-1)
        logits = cumul[:, :, None] - cumul[:, None, :] + in_block[:, None, :]
        logits = jnp.where(causal, logits, -jnp.inf)
        carried = cumul + level[:, None]
        stab = jnp.maximum(carried, jnp.max(logits, axis=-1))
        weights = jnp.exp(logits - stab[:, :, None])
        scores = (
            jnp.einsum("thd,shd->hts", q_block, k_block, preferred_element_type=jnp.float32) * scale
        )
        weighted = (scores * weights).astype(jnp.bfloat16)
        within = jnp.einsum("hts,shv->thv", weighted, v_block, preferred_element_type=jnp.float32)
        earlier = jnp.einsum(
            "thd,hdv->thv", q_block.astype(jnp.float32), memory, precision=lax.Precision.HIGHEST
        )
        earlier = earlier * jnp.exp(carried - stab).T[:, :, None]
        last = cumul[:, -1]
        tail = last[:, None] - cumul + in_block
        level_new = jnp.maximum(last + level, jnp.max(tail, axis=-1))
        tail_weights = jnp.exp(tail - level_new[:, None]) * scale
        scaled_keys = (k_block * tail_weights.T[:, :, None]).astype(jnp.bfloat16)
        memory_new = jnp.exp(last + level - level_new)[:, None, None] * memory
        memory_new = memory_new + jnp.einsum(
            "shd,shv->hdv", scaled_keys, v_block, preferred_element_type=jnp.float32
        )
        return ((memory_new, level_new), (within + earlier, stab))

    init = (
        jnp.zeros((attention_tally, key_size, value_size), jnp.float32),
        jnp.full((attention_tally,), -1e30, jnp.float32),
    )
    (memory_end, level_end), (raw, stabs) = lax.scan(
        advance, init, (queries, keys_all, values_all, incoming_matrix, forgets)
    )
    raw = raw.reshape(rows, attention_tally, value_size)
    stabs = jnp.moveaxis(stabs, 0, 1).reshape(attention_tally, rows)
    running = jnp.cumsum(forget_log, axis=1)
    return (raw, stabs, running, memory_end, level_end, running[:, -1])


def merge_states(earlier, later):
    merged = []
    for group in range(2):
        memory_e, level_e, total_e = earlier[3 * group : 3 * group + 3]
        memory_l, level_l, total_l = later[3 * group : 3 * group + 3]
        level = jnp.maximum(level_e + total_l, level_l)
        memory = (
            jnp.exp(level_e + total_l - level)[:, None, None] * memory_e
            + jnp.exp(level_l - level)[:, None, None] * memory_l
        )
        merged.extend([memory, level, total_e + total_l])
    return tuple(merged)


def finish_group(query, raw, stabs, running, memory_in, level_in, gain, outgate, key_size):
    rows, attention_tally, value_size = raw.shape
    shifted = running + level_in[:, None]
    stab = jnp.maximum(stabs, shifted)
    own = raw * jnp.exp(stabs - stab).T[:, :, None]
    queries = query.reshape(rows, attention_tally, key_size).astype(jnp.float32)
    incoming = jnp.einsum("thd,hdv->thv", queries, memory_in, precision=lax.Precision.HIGHEST)
    total = own + incoming * jnp.exp(shifted - stab).T[:, :, None]
    normal_raw = total * lax.rsqrt(jnp.mean(total * total, axis=-1, keepdims=True) + 1e-06)
    flat = normal_raw.reshape(rows, attention_tally * value_size)
    flat = flat * gain.astype(jnp.float32) * jax.nn.sigmoid(outgate.astype(jnp.float32))
    return flat.astype(jnp.bfloat16)


def norm_rows(middle_f, norm_gain):
    normed = middle_f * lax.rsqrt(jnp.mean(middle_f * middle_f, axis=-1, keepdims=True) + 1e-06)
    return (normed * norm_gain.astype(jnp.float32)).astype(jnp.bfloat16)


def body(
    residual,
    query_wide,
    key_wide,
    value_wide,
    outgate_wide,
    gating_wide,
    gain_wide,
    readout_wide,
    query_narrow,
    key_narrow,
    value_narrow,
    outgate_narrow,
    gating_narrow,
    gain_narrow,
    readout_narrow,
    norm_gain,
    gate_weight,
    up_weight,
    down_weight,
):
    raw_w, stabs_w, running_w, memory_w, level_w, total_w = local_pass(
        query_wide, key_wide, value_wide, gating_wide, DK_A
    )
    raw_n, stabs_n, running_n, memory_n, level_n, total_n = local_pass(
        query_narrow, key_narrow, value_narrow, gating_narrow, DK_B
    )
    carried = entering(
        (memory_w, level_w, total_w, memory_n, level_n, total_n),
        "sp",
        merge_states,
        (
            jnp.zeros_like(memory_w),
            jnp.full_like(level_w, -1e30),
            jnp.zeros_like(total_w),
            jnp.zeros_like(memory_n),
            jnp.full_like(level_n, -1e30),
            jnp.zeros_like(total_n),
        ),
    )
    gated_w = finish_group(
        query_wide, raw_w, stabs_w, running_w, carried[0], carried[1], gain_wide, outgate_wide, DK_A
    )
    gated_n = finish_group(
        query_narrow,
        raw_n,
        stabs_n,
        running_n,
        carried[3],
        carried[4],
        gain_narrow,
        outgate_narrow,
        DK_B,
    )
    mixed = lax.psum_scatter(
        (
            jnp.dot(gated_w, readout_wide, preferred_element_type=jnp.float32)
            + jnp.dot(gated_n, readout_narrow, preferred_element_type=jnp.float32)
        ).astype(jnp.bfloat16),
        "tp",
        scatter_dimension=0,
        tiled=True,
    ).astype(jnp.float32)
    middle_f = (residual.astype(jnp.float32) + mixed).astype(jnp.bfloat16).astype(jnp.float32)
    normed = norm_rows(middle_f, norm_gain)
    all_rows = lax.all_gather(normed, "tp", axis=0, tiled=True)
    gate = jnp.dot(
        all_rows,
        lax.all_gather(gate_weight, "sp", axis=0, tiled=True),
        preferred_element_type=jnp.float32,
    )
    upper = jnp.dot(
        all_rows,
        lax.all_gather(up_weight, "sp", axis=0, tiled=True),
        preferred_element_type=jnp.float32,
    )
    hidden = (jax.nn.silu(gate) * upper).astype(jnp.bfloat16)
    terms = jnp.dot(
        hidden,
        lax.all_gather(down_weight, "sp", axis=1, tiled=True),
        preferred_element_type=jnp.float32,
    )
    back = lax.psum_scatter(
        terms.astype(jnp.bfloat16), "tp", scatter_dimension=0, tiled=True
    ).astype(jnp.float32)
    return (middle_f + back).astype(jnp.bfloat16)


def solution(mesh):
    in_specs = (
        P(("sp", "tp"), None),
        P("sp", "tp"),
        P("sp", "tp"),
        P("sp", "tp"),
        P("sp", "tp"),
        P(None, "tp", "sp"),
        P("tp"),
        P("tp", None),
        P("sp", "tp"),
        P("sp", "tp"),
        P("sp", "tp"),
        P("sp", "tp"),
        P(None, "tp", "sp"),
        P("tp"),
        P("tp", None),
        P(),
        P("sp", "tp"),
        P("sp", "tp"),
        P("tp", "sp"),
    )
    out_specs = P(("sp", "tp"), None)
    return jax.shard_map(body, mesh=mesh, in_specs=in_specs, out_specs=out_specs, check_vma=False)
```

profile of v0, /device:TPU:0, one launch (start us, length us, event | category | flops | bytes accessed | tf_op | source)
XLA Modules:
  0.0 764.9 jit_solution(13011065428079746588)
XLA Ops:
  10.6 5.3 while.55
  19.7 19.3 %while.54 = (s32[]{:T(128)}, f32[4,128,256]{2,1,0:T(8,128)S(1)}, f32[4]{0:T(128)}, f32[2,64,4,256]{3,1,0,2:T(8,128)}, f32[2,4,64]{2,1,0:T(4,128)}, /*index=5*/f3...) while((s32[]{:T(128)}, f32[4,128,256]{2,1,0:T(8,128)S(1)}, ...), condition=%wide.region_4.5_spmd.clone, body=%wide.region_0.4_spmd.clone.sunk | while | flops 130980880 | bytes 3455009 | solution.py:75
  21.8 1.3 add_maximum_fusion.4
  27.8 1.3 fusion.153
  31.8 1.3 add_maximum_fusion.4
  37.8 1.2 fusion.153
  40.0 1.6 copy.70
  41.5 1.3 dynamic-slice
  48.0 44.1 %all-reduce.4 = (f32[64]{0:T(128)S(1)}, f32[64]{0:T(128)S(1)}, f32[64]{0:T(128)S(1)}, f32[64]{0:T(128)S(1)}) all-reduce(f32[64]{0:T(128)S(1)} %dynamic-update-slice, f32[64]{0:T(128)S(1)} %dynamic-update-slice.1, f32[64]{0:T(128)S(1)} %dynamic-update-slice.2, f32[64]{0:T(128)S(1)} %dynamic-update-slice.3), channel_id=2, replica_groups=mesh['sp'=16,'tp'=2] {'sp'}, use_global_device_ids=true, to_apply=%add | all-reduce | flops 256 | bytes 2048
  97.4 1.2 copy.63
  98.7 1.3 convert_element_type.74
  99.9 1.3 convert_element_type.77
  101.2 93.0 %all-gather.18.cloned.1.call-done = f32[64,128,256]{2,1,0:T(8,128)} async-done(((f32[4,128,256]{2,1,0:T(8,128)}), f32[64,128,256]{2,1,0:T(8,128)}) %all-gather.18.cloned.1.call-update) | async-done | bytes 8388624 | tf_op jit(solution)/shard_map/all_gather | solution.py:13
  194.2 56.7 %while.56 = (s32[]{:T(128)}, f32[4,128,256]{2,1,0:T(8,128)S(1)}, f32[4]{0:T(128)}, f32[4,64,128]{2,1,0:T(8,128)S(1)}, f32[4]{0:T(128)}, /*index=5*/s32[]{:T(128)...) while((s32[]{:T(128)}, f32[4,128,256]{2,1,0:T(8,128)S(1)}, ...), condition=%wide.region_13.14_spmd.clone, body=%wide.region_12.13_spmd.clone.sunk | while | flops 819260 | bytes 1966609 | solution.py:25
  194.2 1.3 broadcast_select_fusion.9
  195.5 1.2 fusion.162
  197.8 1.3 broadcast_select_fusion.9
  199.1 1.2 fusion.162
  201.3 1.3 broadcast_select_fusion.9
  202.6 1.2 fusion.162
  204.9 1.3 broadcast_select_fusion.9
  206.2 1.2 fusion.162
  208.4 1.3 broadcast_select_fusion.9
  209.7 1.2 fusion.162
  212.0 1.3 broadcast_select_fusion.9
  215.5 1.3 broadcast_select_fusion.9
  219.1 1.3 broadcast_select_fusion.9
  222.6 1.3 broadcast_select_fusion.9
  226.2 1.3 broadcast_select_fusion.9
  229.7 1.3 broadcast_select_fusion.9
  233.2 1.3 broadcast_select_fusion.9
  236.8 1.3 broadcast_select_fusion.9
  240.3 1.3 broadcast_select_fusion.9
  243.9 1.3 broadcast_select_fusion.9
  247.4 1.3 broadcast_select_fusion.9
  251.8 1.3 multiply_reduce_fusion.1
  254.8 1.5 multiply_reduce_fusion
  256.7 3.0 fusion.76
  259.8 1.3 fusion.67
  262.9 4.4 reduce-scatter.3.cloned.1.call-done
  269.6 2.4 all_gather.52
  272.0 140.6 %all-gather.12.cloned.1.call-done = bf16[2048,2816]{1,0:T(8,128)(2,1)} async-done(((bf16[128,2816]{1,0:T(8,128)(2,1)}), bf16[2048,2816]{1,0:T(8,128)(2,1)}) %all-gather.12.cloned.1.call-update) | async-done | bytes 11534352 | tf_op jit(solution)/shard_map/all_gather | solution.py:185
  412.5 7.1 fusion.118
  419.6 135.2 %all-gather.14.cloned.1.call-done = bf16[2048,2816]{1,0:T(8,128)(2,1)} async-done(((bf16[128,2816]{1,0:T(8,128)(2,1)}), bf16[2048,2816]{1,0:T(8,128)(2,1)}) %all-gather.14.cloned.1.call-update) | async-done | bytes 11534352 | tf_op jit(solution)/shard_map/all_gather | solution.py:190
  554.8 182.8 %all-gather.16.cloned.1.call-done = bf16[2816,2048]{1,0:T(8,128)(2,1)} async-done(((bf16[2816,128]{1,0:T(8,128)(2,1)}), bf16[2816,2048]{1,0:T(8,128)(2,1)}) %all-gather.16.cloned.1.call-update) | async-done | bytes 11534352 | tf_op jit(solution)/shard_map/all_gather | solution.py:196
  737.6 12.4 %convolution_convert_fusion = bf16[128,2048]{1,0:T(8,128)(2,1)} fusion(bf16[2816,2048]{1,0:T(8,128)(2,1)} %all-gather.16.cloned.1.call-done, bf16[128,2048]{1,0:T(8,128)(2,1)S(1)} %all_gather.52, bf16[2048,2816]{1,0:T(8,128)(2,1)} %all-gather.14.cloned.1.call-done, f32[128,2816]{1,0:T(8,128)} %fusion.118), kind=kOutput, calls=%fused_computation.130 | convolution fusion | flops 2955214848 | bytes 25559040 | tf_op jit(solution)/shard_map/dot_general | solution.py:194
  750.0 6.3 reduce-scatter.5.cloned.1.call-done
  756.3 1.7 fusion.75
  (240 shorter events, 74.2 us)
Async XLA Ops:
  6.5 253.2 %copy-start = (bf16[512,2048]{1,0:T(8,128)(2,1)S(1)}, bf16[512,2048]{1,0:T(8,128)(2,1)}, u32[]{:S(2)}) copy-start(bf16[512,2048]{1,0:T(8,128)(2,1)} %param.39) | copy-start | bytes 6291460
  6.5 94.7 %all-gather.20.cloned.1.call-start = ((), (), s32[]{:S(2)}) async-start(), calls=%async_computation.8 | async-start | bytes 2228224 | tf_op jit(solution)/shard_map/all_gather | solution.py:13
  10.6 6.1 copy-start.15
  10.6 7.0 copy-start.8
  10.6 7.1 copy-start.11
  10.6 7.2 copy-start.7
  15.9 0.6 copy-start.3
  15.9 1.6 copy-start.12
  15.9 1.6 copy-start.16
  16.6 177.6 %all-gather.18.cloned.1.call-start = ((), (), s32[]{:S(2)}) async-start(), calls=%async_computation.7 | async-start | bytes 8912896 | tf_op jit(solution)/shard_map/all_gather | solution.py:13
  20.4 2.7 copy-start.6
  21.0 2.1 copy-start.9
  29.8 3.3 copy-start.6
  31.0 2.1 copy-start.9
  39.0 0.8 copy-start.2
  39.9 227.5 %reduce-scatter.3.cloned.1.call-start = ((), (), s32[]{:S(2)}) async-start(), calls=%async_computation.2 | async-start | bytes 786432 | tf_op jit(solution)/shard_map/reduce_scatter | solution.py:171
  46.1 51.3 %copy-start.13 = (f32[4,128]{1,0:T(4,128)}, f32[4,128]{1,0:T(4,128)S(1)}, u32[]{:S(2)}) copy-start(f32[4,128]{1,0:T(4,128)S(1)} %reduce_window_sum.38) | copy-start | bytes 6148
  47.5 49.9 %copy-start.14 = (f32[4,128]{1,0:T(4,128)}, f32[4,128]{1,0:T(4,128)S(1)}, u32[]{:S(2)}) copy-start(f32[4,128]{1,0:T(4,128)S(1)} %reduce_window_sum.39) | copy-start | bytes 6148
  251.0 5.7 copy-start.19
  256.4 3.3 copy-start.10
  256.4 3.3 copy-start.17
  259.7 3.2 copy-start.18
  259.7 7.6 copy-start.4
  261.1 151.4 %all-gather.12.cloned.1.call-start = ((), (), s32[]{:S(2)}) async-start(), calls=%async_computation.3 | async-start | bytes 12255232 | tf_op jit(solution)/shard_map/all_gather | solution.py:185
  261.7 293.1 %all-gather.14.cloned.1.call-start = ((), (), s32[]{:S(2)}) async-start(), calls=%async_computation.4 | async-start | bytes 12255232 | tf_op jit(solution)/shard_map/all_gather | solution.py:190
  262.3 475.3 %all-gather.16.cloned.1.call-start = ((), (), s32[]{:S(2)}) async-start(), calls=%async_computation.5 | async-start | bytes 12255232 | tf_op jit(solution)/shard_map/all_gather | solution.py:196
  262.8 493.5 %reduce-scatter.5.cloned.1.call-start = ((), (), s32[]{:S(2)}) async-start(), calls=%async_computation.6 | async-start | bytes 786432 | tf_op jit(solution)/shard_map/reduce_scatter | solution.py:199
  419.6 336.7 %copy-start.5 = (bf16[64,2048]{1,0:T(8,128)(2,1)S(1)}, bf16[64,2048]{1,0:T(8,128)(2,1)}, u32[]{:S(2)}) copy-start(bf16[64,2048]{1,0:T(8,128)(2,1)} %reduce-scatter.3.cloned.1.call-done) | copy-start | bytes 786436
  737.6 20.5 %copy-start.1 = (bf16[512,2048]{1,0:T(8,128)(2,1)S(1)}, bf16[512,2048]{1,0:T(8,128)(2,1)}, u32[]{:S(2)}) copy-start(bf16[512,2048]{1,0:T(8,128)(2,1)} %param.39) | copy-start | bytes 6291460
Sparse Core Ops, SparseCore 0:
  16.7 63.6 all-gather.19
  83.2 111.0 all-gather.17
  261.2 6.0 reduce-scatter.2
  270.0 142.5 all-gather.11
  415.1 139.5 all-gather.13
  557.3 180.2 all-gather.15
  750.2 6.0 reduce-scatter.4
where the time goes:
time: 768 us; the launch traced here: 765 us
  waiting for transfers between devices  564 us (73%)
  other arithmetic  79.1 us (10%)
  blocking collectives  46.5 us (6%)
  matrix products  35.6 us (5%)
  local copies, waits for them, and re-layouts  24.3 us (3%)
  between operations  14.5 us (2%)
    all_gather x1, waiting for transfers between devices, body(): lax.all_gather(down_weight, 'sp', axis=1, tiled=True)  183 us
    all_gather x1, waiting for transfers between devices, body(): lax.all_gather(gate_weight, 'sp', axis=0, tiled=True)  141 us
    all_gather x1, waiting for transfers between devices, body(): lax.all_gather(up_weight, 'sp', axis=0, tiled=True)  135 us
    all_gather x2, waiting for transfers between devices, entering(): everything = jax.tree.map(lambda part: lax.all_gather(part, axis), value)  93 us
    select_n x48, other arithmetic, step(): return jax.tree.map(lambda a, b: jnp.where(reached, a, b), new, before)  55.7 us
    unnamed x1, blocking collectives  44.1 us
  transfers between devices with their start and end apart: 7, of which 6 were waited for; matrix products, arithmetic and copies ran while one was open for 6% of the time, Pallas kernels for 0%

commit v1 on v0

--- a/solution.py
+++ b/solution.py
@@ -6,6 +6,12 @@
 DK_A = 128
 DK_B = 64
 BLOCK = 64
+
+
+def all_parts(block, name, d):
+    pieces = lax.all_gather(block, name, axis=0, tiled=False)
+    whole = jnp.concatenate(pieces, axis=d)
+    return whole
 
 
 def entering(value, axis, combine, identity):
@@ -191,11 +197,7 @@
         preferred_element_type=jnp.float32,
     )
     hidden = (jax.nn.silu(gate) * upper).astype(jnp.bfloat16)
-    terms = jnp.dot(
-        hidden,
-        lax.all_gather(down_weight, "sp", axis=1, tiled=True),
-        preferred_element_type=jnp.float32,
-    )
+    terms = jnp.dot(hidden, all_parts(down_weight, "sp", 1), preferred_element_type=jnp.float32)
     back = lax.psum_scatter(
         terms.astype(jnp.bfloat16), "tp", scatter_dimension=0, tiled=True
     ).astype(jnp.float32)

time: 768 us -> 729 us (0.949)
  waiting for transfers between devices: 564 us -> 508 us
  local copies, waits for them, and re-layouts: 24.3 us -> 40.4 us
    all_gather x1, waiting for transfers between devices: 183 us -> 141 us  [all_parts(): pieces = lax.all_gather(block, name, axis=0, tiled=False)]
    reshape x0 -> x1, local copies, waits for them, and re-layouts: none -> 15.2 us  [all_parts(): whole = jnp.concatenate(pieces, axis=d)]
    all_gather x1, waiting for transfers between devices: 141 us -> 127 us  [body(): lax.all_gather(gate_weight, 'sp', axis=0, tiled=True)]
  transfers between devices with their start and end apart: 7 -> 7, of which waited for: 6 -> 6; matrix products, arithmetic and copies ran while one was open for 6% -> 9% of each run, Pallas kernels for 0% -> 0%
where the time goes in v1:
time: 729 us; the launch traced here: 726 us
  waiting for transfers between devices  508 us (70%)
  other arithmetic  79.6 us (11%)
  blocking collectives  46.2 us (6%)
  local copies, waits for them, and re-layouts  40.4 us (6%)
  matrix products  36.9 us (5%)
  between operations  14.5 us (2%)
    all_gather x1, waiting for transfers between devices, all_parts(): pieces = lax.all_gather(block, name, axis=0, tiled=False)  141 us
    all_gather x1, waiting for transfers between devices, body(): lax.all_gather(up_weight, 'sp', axis=0, tiled=True)  135 us
    all_gather x1, waiting for transfers between devices, body(): lax.all_gather(gate_weight, 'sp', axis=0, tiled=True)  127 us
    all_gather x2, waiting for transfers between devices, entering(): everything = jax.tree.map(lambda part: lax.all_gather(part, axis), value)  92.5 us
    select_n x48, other arithmetic, step(): return jax.tree.map(lambda a, b: jnp.where(reached, a, b), new, before)  56.2 us
    unnamed x1, blocking collectives  43.8 us
    reshape x1, local copies, waits for them, and re-layouts, all_parts(): whole = jnp.concatenate(pieces, axis=d)  15.2 us
  transfers between devices with their start and end apart: 7, of which 6 were waited for; matrix products, arithmetic and copies ran while one was open for 9% of the time, Pallas kernels for 0%

profile of v1, /device:TPU:0, one launch (start us, length us, event | category | flops | bytes accessed | tf_op | source)
XLA Modules:
  0.0 726.2 jit_solution(2016900786363241189)
XLA Ops:
  10.6 5.3 while.55
  20.6 19.5 %while.54 = (s32[]{:T(128)}, f32[4,128,256]{2,1,0:T(8,128)S(1)}, f32[4]{0:T(128)}, f32[2,64,4,256]{3,1,0,2:T(8,128)}, f32[2,4,64]{2,1,0:T(4,128)}, /*index=5*/f3...) while((s32[]{:T(128)}, f32[4,128,256]{2,1,0:T(8,128)S(1)}, ...), condition=%wide.region_4.5_spmd.clone, body=%wide.region_0.4_spmd.clone.sunk | while | flops 130980880 | bytes 3455009 | solution.py:81
  22.7 1.3 add_maximum_fusion.4
  28.7 1.3 fusion.153
  32.7 1.3 add_maximum_fusion.4
  38.7 1.3 fusion.153
  41.0 1.6 copy.93
  42.6 1.2 dynamic-slice
  48.9 43.8 %all-reduce.4 = (f32[64]{0:T(128)S(1)}, f32[64]{0:T(128)S(1)}, f32[64]{0:T(128)S(1)}, f32[64]{0:T(128)S(1)}) all-reduce(f32[64]{0:T(128)S(1)} %dynamic-update-slice, f32[64]{0:T(128)S(1)} %dynamic-update-slice.1, f32[64]{0:T(128)S(1)} %dynamic-update-slice.2, f32[64]{0:T(128)S(1)} %dynamic-update-slice.3), channel_id=2, replica_groups=mesh['sp'=16,'tp'=2] {'sp'}, use_global_device_ids=true, to_apply=%add | all-reduce | flops 256 | bytes 2048
  98.1 1.2 copy.86
  99.3 1.3 convert_element_type.74
  100.6 1.2 convert_element_type.77
  101.8 92.5 %all-gather.17.cloned.1.call-done = f32[64,128,256]{2,1,0:T(8,128)} async-done(((f32[4,128,256]{2,1,0:T(8,128)}), f32[64,128,256]{2,1,0:T(8,128)}) %all-gather.17.cloned.1.call-update) | async-done | bytes 8388624 | tf_op jit(solution)/shard_map/all_gather | solution.py:19
  194.3 57.2 %while.56 = (s32[]{:T(128)}, f32[4,128,256]{2,1,0:T(8,128)S(1)}, f32[4]{0:T(128)}, f32[4,64,128]{2,1,0:T(8,128)S(1)}, f32[4]{0:T(128)}, /*index=5*/s32[]{:T(128)...) while((s32[]{:T(128)}, f32[4,128,256]{2,1,0:T(8,128)S(1)}, ...), condition=%wide.region_13.14_spmd.clone, body=%wide.region_12.13_spmd.clone.sunk | while | flops 819260 | bytes 1966609 | solution.py:31
  194.3 1.3 broadcast_select_fusion.9
  197.9 1.3 broadcast_select_fusion.9
  201.5 1.3 broadcast_select_fusion.9
  205.1 1.3 broadcast_select_fusion.9
  208.7 1.3 broadcast_select_fusion.9
  212.2 1.3 broadcast_select_fusion.9
  215.8 1.3 broadcast_select_fusion.9
  219.4 1.3 broadcast_select_fusion.9
  220.8 1.2 fusion.162
  223.0 1.3 broadcast_select_fusion.9
  226.6 1.3 broadcast_select_fusion.9
  230.2 1.3 broadcast_select_fusion.9
  233.7 1.3 broadcast_select_fusion.9
  237.3 1.3 broadcast_select_fusion.9
  238.6 1.2 fusion.162
  240.9 1.3 broadcast_select_fusion.9
  242.2 1.2 fusion.162
  244.4 1.3 broadcast_select_fusion.9
  245.7 1.2 fusion.162
  248.0 1.3 broadcast_select_fusion.9
  252.3 1.3 multiply_reduce_fusion.1
  255.4 1.5 multiply_reduce_fusion
  257.2 3.0 fusion.76
  260.3 1.3 fusion.67
  263.5 4.4 reduce-scatter.3.cloned.1.call-done
  270.2 2.4 all_gather.55
  272.5 140.6 %all-gather.21.cloned.1.call-done = bf16[45056,128]{1,0:T(8,128)(2,1)} async-done(((bf16[2816,128]{1,0:T(8,128)(2,1)}), bf16[45056,128]{1,0:T(8,128)(2,1)}) %all-gather.21.cloned.1.call-update) | async-done | bytes 11534352 | tf_op jit(solution)/shard_map/all_gather | solution.py:12
  413.1 15.2 %copy.95 = bf16[2816,16,128]{0,2,1:T(8,128)(2,1)} copy(bf16[2816,16,128]{2,0,1:T(8,128)(2,1)} %bitcast.311) | data formatting | bytes 23068672 | tf_op jit(solution)/shard_map/reshape | solution.py:13
  428.3 127.0 %all-gather.13.cloned.1.call-done = bf16[2048,2816]{1,0:T(8,128)(2,1)} async-done(((bf16[128,2816]{1,0:T(8,128)(2,1)}), bf16[2048,2816]{1,0:T(8,128)(2,1)}) %all-gather.13.cloned.1.call-update) | async-done | bytes 11534352 | tf_op jit(solution)/shard_map/all_gather | solution.py:191
  555.3 7.1 fusion.118
  562.4 135.2 %all-gather.15.cloned.1.call-done = bf16[2048,2816]{1,0:T(8,128)(2,1)} async-done(((bf16[128,2816]{1,0:T(8,128)(2,1)}), bf16[2048,2816]{1,0:T(8,128)(2,1)}) %all-gather.15.cloned.1.call-update) | async-done | bytes 11534352 | tf_op jit(solution)/shard_map/all_gather | solution.py:196
  697.6 13.8 %convolution_convert_fusion = bf16[128,2048]{1,0:T(8,128)(2,1)} fusion(bf16[2816,2048]{0,1:T(8,128)(2,1)} %bitcast.312, bf16[128,2048]{1,0:T(8,128)(2,1)S(1)} %all_gather.55, bf16[2048,2816]{1,0:T(8,128)(2,1)} %all-gather.15.cloned.1.call-done, f32[128,2816]{1,0:T(8,128)} %fusion.118), kind=kOutput, calls=%fused_computation.130 | convolution fusion | flops 2955214848 | bytes 25559040 | tf_op jit(solution)/shard_map/dot_general | solution.py:200
  711.4 6.3 reduce-scatter.5.cloned.1.call-done
  717.6 1.7 fusion.75
  (239 shorter events, 76.4 us)
Async XLA Ops:
  6.5 253.8 %copy-start = (bf16[512,2048]{1,0:T(8,128)(2,1)S(1)}, bf16[512,2048]{1,0:T(8,128)(2,1)}, u32[]{:S(2)}) copy-start(bf16[512,2048]{1,0:T(8,128)(2,1)} %param.39) | copy-start | bytes 6291460
  6.5 95.3 %all-gather.19.cloned.1.call-start = ((), (), s32[]{:S(2)}) async-start(), calls=%async_computation.7 | async-start | bytes 2228224 | tf_op jit(solution)/shard_map/all_gather | solution.py:19
  10.6 6.1 copy-start.14
  10.6 6.9 copy-start.8
  10.6 8.1 %copy-start.7 = (bf16[128,512]{1,0:T(8,128)(2,1)S(1)}, bf16[128,512]{1,0:T(8,128)(2,1)}, u32[]{:S(2)}) copy-start(bf16[128,512]{1,0:T(8,128)(2,1)} %param.26) | copy-start | bytes 393220
  15.9 0.6 copy-start.3
  15.9 4.6 copy-start.11
  15.9 4.6 copy-start.15
  16.6 177.7 %all-gather.17.cloned.1.call-start = ((), (), s32[]{:S(2)}) async-start(), calls=%async_computation.6 | async-start | bytes 8912896 | tf_op jit(solution)/shard_map/all_gather | solution.py:19
  21.3 2.7 copy-start.6
  21.9 2.0 copy-start.9
  30.7 3.3 copy-start.6
  32.0 2.0 copy-start.9
  40.1 0.8 copy-start.2
  40.9 227.0 %reduce-scatter.3.cloned.1.call-start = ((), (), s32[]{:S(2)}) async-start(), calls=%async_computation.2 | async-start | bytes 786432 | tf_op jit(solution)/shard_map/reduce_scatter | solution.py:177
  47.0 51.0 %copy-start.12 = (f32[4,128]{1,0:T(4,128)}, f32[4,128]{1,0:T(4,128)S(1)}, u32[]{:S(2)}) copy-start(f32[4,128]{1,0:T(4,128)S(1)} %reduce_window_sum.38) | copy-start | bytes 6148
  48.5 49.6 %copy-start.13 = (f32[4,128]{1,0:T(4,128)}, f32[4,128]{1,0:T(4,128)S(1)}, u32[]{:S(2)}) copy-start(f32[4,128]{1,0:T(4,128)S(1)} %reduce_window_sum.39) | copy-start | bytes 6148
  251.5 5.7 copy-start.18
  256.9 3.4 copy-start.10
  257.0 3.4 copy-start.16
  260.3 3.1 copy-start.17
  260.3 7.6 %copy-start.4 = (bf16[64,2048]{1,0:T(8,128)(2,1)S(1)}, bf16[64,2048]{1,0:T(8,128)(2,1)}, u32[]{:S(2)}) copy-start(bf16[64,2048]{1,0:T(8,128)(2,1)} %param.25) | copy-start | bytes 786436
  261.7 151.4 %all-gather.21.cloned.1.call-start = ((), (), s32[]{:S(2)}) async-start(), calls=%async_computation.8 | async-start | bytes 12255232 | tf_op jit(solution)/shard_map/all_gather | solution.py:12
  262.2 293.1 %all-gather.13.cloned.1.call-start = ((), (), s32[]{:S(2)}) async-start(), calls=%async_computation.3 | async-start | bytes 12255232 | tf_op jit(solution)/shard_map/all_gather | solution.py:191
  262.8 434.7 %all-gather.15.cloned.1.call-start = ((), (), s32[]{:S(2)}) async-start(), calls=%async_computation.4 | async-start | bytes 12255232 | tf_op jit(solution)/shard_map/all_gather | solution.py:196
  263.4 454.2 %reduce-scatter.5.cloned.1.call-start = ((), (), s32[]{:S(2)}) async-start(), calls=%async_computation.5 | async-start | bytes 786432 | tf_op jit(solution)/shard_map/reduce_scatter | solution.py:201
  697.6 20.1 %copy-start.5 = (bf16[64,2048]{1,0:T(8,128)(2,1)S(1)}, bf16[64,2048]{1,0:T(8,128)(2,1)}, u32[]{:S(2)}) copy-start(bf16[64,2048]{1,0:T(8,128)(2,1)} %reduce-scatter.3.cloned.1.call-done) | copy-start | bytes 786436
  697.6 21.8 %copy-start.1 = (bf16[512,2048]{1,0:T(8,128)(2,1)S(1)}, bf16[512,2048]{1,0:T(8,128)(2,1)}, u32[]{:S(2)}) copy-start(bf16[512,2048]{1,0:T(8,128)(2,1)} %param.39) | copy-start | bytes 6291460
Sparse Core Ops, SparseCore 0:
  16.7 63.6 all-gather.18
  83.2 111.0 all-gather.16
  261.8 6.0 reduce-scatter.2
  270.5 142.5 all-gather.20
  415.7 139.5 all-gather.12
  557.9 139.5 all-gather.14
  711.5 6.0 reduce-scatter.4
